TPU v7x, 32 devices: a whole 2x2x4 slice. The times are simulated.
32 devices in a mesh: ep: 8 (over z, core), tp: 4 (over y, x).
Axes of the slice: x: 2, y: 2, z: 4, core: 2. Of those that a mesh axis runs over, the one named last changes fastest.
Arguments:
- tokens: bfloat16 [2048, 2048], P('ep'), may hold values from -6 to 6
- gate_proj: bfloat16 [8, 2048, 4096], P('ep', None, 'tp'), may hold values from -0.125 to 0.125
- up_proj: bfloat16 [8, 2048, 4096], P('ep', None, 'tp'), may hold values from -0.125 to 0.125
- down_proj: bfloat16 [8, 4096, 2048], P('ep', 'tp'), may hold values from -0.09375 to 0.09375
- side_input_weight: bfloat16 [2048, 1024], P(None, 'tp'), may hold values from -0.125 to 0.125
- dense_out: bfloat16 [1024, 2048], P(None, 'tp'), may hold values from -0.1875 to 0.1875
- dense_gate: bfloat16 [2048], replicated, may hold values from -0.125 to 0.125
- chosen_rows: int32 [8, 256], P(None, 'ep'), may hold values from 0 to 255, as said below
- choice_weights: float32 [8, 256], P(None, 'ep'), may hold values from 0.25 to 1
Outputs:
- mixed: bfloat16 [2048, 2048], P('ep', 'tp')
Inputs may be any that keep to these rules, and one draw needn't show every extreme that they name: `chosen_rows`: for each expert and each block of 32 columns (one index of ep), the 32 rows are distinct rows of that index's 256 tokens; every expert reads exactly 32 tokens of every index.
All inputs are finite; a program needn't handle non-finite values.
Results may differ from a plain program's by a relative error of at most 0.015.
Values may be sent and summed in bfloat16 or wider, within the bound.
No kernel may reach another device: no remote copies, remote signals or barrier semaphores. Data moves between devices by JAX's collectives and lax.ppermute only.
A program may use at most 64 MiB of HBM per device.

v0:
```python
import jax
import jax.numpy as jnp
from jax import lax
from jax.sharding import PartitionSpec as P


def per_device(
    tokens,
    gate_proj,
    up_proj,
    down_proj,
    side_input_weight,
    dense_out,
    dense_gate,
    chosen_rows,
    choice_weights,
):
    tok_rows = tokens.shape[0]
    width = tokens.shape[1] // lax.axis_size("tp")
    column_position = lax.axis_index("tp") * width
    own_cols = lax.dynamic_slice_in_dim(tokens, column_position, width, 1)
    expert_count, slot_rows = chosen_rows.shape
    capacity = expert_count * slot_rows
    picked = jnp.take(own_cols, chosen_rows.reshape(-1), axis=0).reshape(
        expert_count, slot_rows, width
    )
    arrived = lax.all_to_all(picked, "ep", split_axis=0, concat_axis=1, tiled=True).reshape(
        capacity, width
    )
    w_gate = gate_proj[0]
    w_up = up_proj[0]
    w_down = down_proj[0]
    piece = lax.all_gather(arrived, "tp", axis=1, tiled=True)
    gate_val = jnp.dot(piece, w_gate, preferred_element_type=jnp.float32)
    up_val = jnp.dot(piece, w_up, preferred_element_type=jnp.float32)
    hidden = (jax.nn.silu(gate_val) * up_val).astype(jnp.bfloat16)
    summed = lax.psum_scatter(
        lax.dot_general(
            w_down, hidden, (((0,), (1,)), ((), ())), preferred_element_type=jnp.float32
        ).astype(jnp.bfloat16),
        "tp",
        scatter_dimension=0,
        tiled=True,
    )
    returned = lax.all_to_all(summed, "ep", split_axis=1, concat_axis=1, tiled=True)
    hits = (
        chosen_rows.reshape(-1)[:, None] == jnp.arange(tok_rows, dtype=jnp.int32)[None, :]
    ).astype(jnp.bfloat16)
    scaled = returned.astype(jnp.float32) * choice_weights.reshape(-1)[None, :]
    high_part = scaled.astype(jnp.bfloat16)
    lower_half = (scaled - high_part.astype(jnp.float32)).astype(jnp.bfloat16)
    contract = (((0,), (1,)), ((), ()))
    routed = lax.dot_general(
        hits, high_part, contract, preferred_element_type=jnp.float32
    ) + lax.dot_general(hits, lower_half, contract, preferred_element_type=jnp.float32)
    dense_hidden = jax.nn.silu(
        jnp.dot(tokens, side_input_weight, preferred_element_type=jnp.float32)
    ).astype(jnp.bfloat16)
    dense_val = jnp.dot(
        lax.all_gather(dense_hidden, "tp", axis=1, tiled=True),
        dense_out,
        preferred_element_type=jnp.float32,
    )
    side_gate = jax.nn.sigmoid(jnp.dot(tokens, dense_gate, preferred_element_type=jnp.float32))
    return (routed + side_gate[:, None] * dense_val).astype(jnp.bfloat16)


def solution(mesh):
    placed = (
        P("ep", None),
        P("ep", None, "tp"),
        P("ep", None, "tp"),
        P("ep", "tp", None),
        P(None, "tp"),
        P(None, "tp"),
        P(),
        P(None, "ep"),
        P(None, "ep"),
    )
    return jax.shard_map(
        per_device, mesh=mesh, in_specs=placed, out_specs=P("ep", "tp"), check_vma=False
    )
```

profile of v0, /device:TPU:0, one launch (start us, length us, event | category | flops | bytes accessed | tf_op | source)
XLA Modules:
  0.0 116.5 jit_solution(18036005292770435474)
XLA Ops:
  6.5 0.9 reshape.57
  7.4 0.7 compare_and_fusion
  8.1 1.2 gather_fusion
  9.3 0.1 broadcast_select_fusion
  9.4 16.0 %all_to_all.18 = bf16[8,32,512]{2,1,0:T(8,128)(2,1)} all-to-all(bf16[8,32,512]{2,1,0:T(8,128)(2,1)S(1)} %broadcast_select_fusion), channel_id=1, replica_groups=mesh['ep'=8,'tp'=4] {'ep'}, dimensions={0} | all-to-all | bytes 524288 | tf_op jit(solution)/shard_map/all_to_all | solution.py:27
  25.4 0.0 all-gather.2.cloned.1.call-update
  25.4 0.0 reduce-scatter.2.cloned.1.call-start
  25.4 25.4 %all-gather.2.cloned.1.call-done = bf16[256,2048]{1,0:T(8,128)(2,1)} async-done(((bf16[256,512]{1,0:T(8,128)(2,1)}), bf16[256,2048]{1,0:T(8,128)(2,1)}) %all-gather.2.cloned.1.call-update) | async-done | bytes 1048592 | tf_op jit(solution)/shard_map/all_gather | solution.py:33
  50.9 3.8 %fusion.4 = f32[256,1024]{1,0:T(8,128)S(1)} fusion(bf16[256,2048]{1,0:T(8,128)(2,1)} %all-gather.2.cloned.1.call-done, bf16[1,2048,1024]{2,1,0:T(8,128)(2,1)} %param.10), kind=kOutput, calls=%fused_computation.5 | convolution fusion | flops 1073741824 | bytes 6291456 | tf_op jit(solution)/shard_map/dot_general | solution.py:34
  54.7 0.0 copy-start.2
  54.7 6.9 %fusion.9 = bf16[2048,256]{0,1:T(8,128)(2,1)} fusion(bf16[1,1024,2048]{2,1,0:T(8,128)(2,1)} %param.12, bf16[256,2048]{1,0:T(8,128)(2,1)S(1)} %copy-done.5, bf16[1,2048,1024]{2,1,0:T(8,128)(2,1)} %param.11, f32[256,1024]{1,0:T(8,128)S(1)} %fusion.4), kind=kOutput, calls=%fused_computation.8 | convolution fusion | flops 2149580800 | bytes 11534336 | tf_op jit(solution)/shard_map/dot_general | solution.py:38
  61.7 0.0 reduce-scatter.2.cloned.1.call-update
  61.7 0.1 eq.15
  61.8 0.1 mul.35
  61.9 1.8 %multiply_convert_fusion = bf16[256,256]{1,0:T(8,128)(2,1)S(1)} fusion(bf16[256,2048]{1,0:T(8,128)(2,1)S(1)} %copy-done, bf16[2048,256]{1,0:T(8,128)(2,1)} %param.13), kind=kOutput, calls=%fused_computation.20 | convolution fusion | flops 268763136 | bytes 2228224 | tf_op jit(solution)/shard_map/dot_general | solution.py:57
  63.6 17.9 %all_gather.7 = bf16[256,1024]{1,0:T(8,128)(2,1)S(1)} all-gather(bf16[256,256]{1,0:T(8,128)(2,1)S(1)} %multiply_convert_fusion), channel_id=1, replica_groups=mesh['ep'=8,'tp'=4] {'tp'}, dimensions={1}, use_global_device_ids=true | all-gather | bytes 655360 | tf_op jit(solution)/shard_map/all_gather | solution.py:60
  81.6 11.8 %reduce-scatter.2.cloned.1.call-done = bf16[512,256]{0,1:T(8,128)(2,1)} async-done(((bf16[2048,256]{0,1:T(8,128)(2,1)}), bf16[512,256]{0,1:T(8,128)(2,1)}) %reduce-scatter.2.cloned.1.call-update) | async-done | bytes 262160 | tf_op jit(solution)/shard_map/reduce_scatter | solution.py:37
  93.3 4.6 %all-to-all-start.1 = ((bf16[512,8,32]{0,2,1:T(8,128)(2,1)}), bf16[512,8,32]{0,2,1:T(8,128)(2,1)S(1)}, u32[]{:S(2)}, u32[]{:S(2)}) async-start(bf16[512,8,32]{0,2,1:T(8,128)(2,1)} %bitcast.41), calls=%async_computation.2 | async-start | bytes 524288 | tf_op jit(solution)/shard_map/all_to_all | solution.py:45
  97.9 0.4 fusion.32
  98.3 9.3 %all-to-all-done.1 = bf16[512,8,32]{0,2,1:T(8,128)(2,1)S(1)} async-done(((bf16[512,8,32]{0,2,1:T(8,128)(2,1)}), bf16[512,8,32]{0,2,1:T(8,128)(2,1)S(1)}, u32[]{:S(2)}, u32[]{:S(2)}) %all-to-all-start.1) | async-done | bytes 262176 | tf_op jit(solution)/shard_map/all_to_all | solution.py:45
  107.7 0.1 fusion.23
  107.8 0.3 fusion.28
  108.1 0.4 convolution_add_fusion
  108.5 1.1 fusion.19
  (17 shorter events, 0.1 us)
Async XLA Ops:
  6.5 1.6 %copy-start = (bf16[256,2048]{1,0:T(8,128)(2,1)S(1)}, bf16[256,2048]{1,0:T(8,128)(2,1)}, u32[]{:S(2)}) copy-start(bf16[256,2048]{1,0:T(8,128)(2,1)} %param.9) | copy-start | bytes 3145732
  6.5 44.3 %all-gather.2.cloned.1.call-start = ((), (), s32[]{:S(2)}) async-start(), calls=%async_computation.3 | async-start | bytes 1310720 | tf_op jit(solution)/shard_map/all_gather | solution.py:33
  25.4 67.9 %reduce-scatter.2.cloned.1.call-start = ((), (), s32[]{:S(2)}) async-start(), calls=%async_computation.4 | async-start | bytes 1310720 | tf_op jit(solution)/shard_map/reduce_scatter | solution.py:37
  50.9 3.8 %copy-start.5 = (bf16[256,2048]{1,0:T(8,128)(2,1)S(1)}, bf16[256,2048]{1,0:T(8,128)(2,1)}, u32[]{:S(2)}) copy-start(bf16[256,2048]{1,0:T(8,128)(2,1)} %all-gather.2.cloned.1.call-done) | copy-start | bytes 3145732
  54.7 7.0 %copy-start.2 = (s32[8,32]{1,0:T(8,128)S(1)}, s32[8,32]{1,0:T(8,128)}, u32[]{:S(2)}) copy-start(s32[8,32]{1,0:T(8,128)} %param.16) | copy-start | bytes 3076
  54.7 7.0 %copy-start.4 = (f32[8,32]{1,0:T(8,128)S(1)}, f32[8,32]{1,0:T(8,128)}, u32[]{:S(2)}) copy-start(f32[8,32]{1,0:T(8,128)} %param.17) | copy-start | bytes 3076
  54.7 7.1 %copy-start.3 = (bf16[2048]{0:T(1024)(128)(2,1)S(1)}, bf16[2048]{0:T(1024)(128)(2,1)}, u32[]{:S(2)}) copy-start(bf16[2048]{0:T(1024)(128)(2,1)} %param.15) | copy-start | bytes 12292
  61.9 46.7 %copy-start.1 = (bf16[1024,512]{1,0:T(8,128)(2,1)S(1)}, bf16[1024,512]{1,0:T(8,128)(2,1)}, u32[]{:S(2)}) copy-start(bf16[1024,512]{1,0:T(8,128)(2,1)} %param.14) | copy-start | bytes 3145732
  93.3 14.3 %all-to-all-start.1 = ((bf16[512,8,32]{0,2,1:T(8,128)(2,1)}), bf16[512,8,32]{0,2,1:T(8,128)(2,1)S(1)}, u32[]{:S(2)}, u32[]{:S(2)}) async-start(bf16[512,8,32]{0,2,1:T(8,128)(2,1)} %bitcast.41), calls=%async_computation.2 | async-start | bytes 524288 | tf_op jit(solution)/shard_map/all_to_all | solution.py:45
Sparse Core Ops, SparseCore 0:
  25.5 25.2 all-gather.1
  61.8 31.4 reduce-scatter.1
where the time goes:
time: 117 us
  waiting for transfers between devices  46.5 us (40%)
  blocking collectives  33.9 us (29%)
  matrix products  14.8 us (13%)
  between operations  13.5 us (12%)
  starting transfers between devices  4.65 us (4%)
  local copies, waits for them, and re-layouts  2.23 us (2%)
    all_gather x1, waiting for transfers between devices, per_device(): piece = lax.all_gather(arrived, 'tp', axis=1, tiled=True)  25.4 us
    all_gather x1, blocking collectives, per_device(): lax.all_gather(dense_hidden, 'tp', axis=1, tiled=True)  17.9 us
    all_to_all x1, blocking collectives, per_device(): lax.all_to_all(picked, 'ep', split_axis=0, concat_axis=1, tiled=True)  16 us
    reduce_scatter x1, waiting for transfers between devices, per_device(): lax.psum_scatter(lax.dot_general(w_down, hidden, (((0,), (1,)), ((), ()))...  11.8 us
    all_to_all x1, waiting for transfers between devices, per_device(): lax.all_to_all(summed, 'ep', split_axis=1, concat_axis=1, tiled=True)  9.33 us
    dot_general x1, matrix products, per_device(): lax.dot_general(w_down, hidden, (((0,), (1,)), ((), ())), preferred_eleme...  6.9 us
    all_to_all x1, starting transfers between devices, per_device(): lax.all_to_all(summed, 'ep', split_axis=1, concat_axis=1, tiled=True)  4.61 us
    dot_general x1, matrix products, per_device(): gate_val = jnp.dot(piece, w_gate, preferred_element_type=jnp.float32)  3.83 us
  transfers between devices with their start and end apart: 3, of which 3 were waited for; matrix products, arithmetic and copies ran while one was open for 2% of the time, Pallas kernels for 0%

commit v1 on v0

--- a/solution.py
+++ b/solution.py
@@ -30,7 +30,7 @@
     w_gate = gate_proj[0]
     w_up = up_proj[0]
     w_down = down_proj[0]
-    piece = lax.all_gather(arrived, "tp", axis=1, tiled=True)
+    piece = jnp.concatenate(lax.all_gather(arrived, "tp"), axis=1)
     gate_val = jnp.dot(piece, w_gate, preferred_element_type=jnp.float32)
     up_val = jnp.dot(piece, w_up, preferred_element_type=jnp.float32)
     hidden = (jax.nn.silu(gate_val) * up_val).astype(jnp.bfloat16)

time: 117 us -> 118 us (level)
  local copies, waits for them, and re-layouts: 2.23 us -> 3.7 us
    all_gather x0 -> x1, local copies, waits for them, and re-layouts: none -> 1.47 us  [per_device(): piece = jnp.concatenate(lax.all_gather(arrived, 'tp'), axis=1)]
where the time goes in v1:
time: 118 us
  waiting for transfers between devices  46.7 us (40%)
  blocking collectives  33.9 us (29%)
  matrix products  14.4 us (12%)
  between operations  13.5 us (11%)
  starting transfers between devices  4.66 us (4%)
  local copies, waits for them, and re-layouts  3.7 us (3%)
    all_gather x1, waiting for transfers between devices, per_device(): piece = jnp.concatenate(lax.all_gather(arrived, 'tp'), axis=1)  25.5 us
    all_gather x1, blocking collectives, per_device(): lax.all_gather(dense_hidden, 'tp', axis=1, tiled=True)  17.9 us
    all_to_all x1, blocking collectives, per_device(): lax.all_to_all(picked, 'ep', split_axis=0, concat_axis=1, tiled=True)  16 us
    reduce_scatter x1, waiting for transfers between devices, per_device(): lax.psum_scatter(lax.dot_general(w_down, hidden, (((0,), (1,)), ((), ()))...  11.8 us
    all_to_all x1, waiting for transfers between devices, per_device(): lax.all_to_all(summed, 'ep', split_axis=1, concat_axis=1, tiled=True)  9.33 us
    dot_general x1, matrix products, per_device(): lax.dot_general(w_down, hidden, (((0,), (1,)), ((), ())), preferred_eleme...  6.93 us
    all_to_all x1, starting transfers between devices, per_device(): lax.all_to_all(summed, 'ep', split_axis=1, concat_axis=1, tiled=True)  4.61 us
    dot_general x1, matrix products, per_device(): gate_val = jnp.dot(piece, w_gate, preferred_element_type=jnp.float32)  3.46 us
  transfers between devices with their start and end apart: 3, of which 3 were waited for; matrix products, arithmetic and copies ran while one was open for 2% of the time, Pallas kernels for 0%

profile of v1, /device:TPU:0, one launch (start us, length us, event | category | flops | bytes accessed | tf_op | source)
XLA Modules:
  0.0 117.8 jit_solution(2439496366504698470)
XLA Ops:
  6.5 0.9 reshape.59
  7.4 0.7 compare_and_fusion
  8.1 1.2 gather_fusion
  9.3 0.1 broadcast_select_fusion
  9.4 16.0 %all_to_all.21 = bf16[8,32,512]{2,1,0:T(8,128)(2,1)} all-to-all(bf16[8,32,512]{2,1,0:T(8,128)(2,1)S(1)} %broadcast_select_fusion), channel_id=1, replica_groups=mesh['ep'=8,'tp'=4] {'ep'}, dimensions={0} | all-to-all | bytes 524288 | tf_op jit(solution)/shard_map/all_to_all | solution.py:27
  25.4 0.0 all-gather.2.cloned.1.call-update
  25.4 0.0 reduce-scatter.2.cloned.1.call-start
  25.4 25.5 %all-gather.2.cloned.1.call-done = bf16[4,256,512]{2,1,0:T(8,128)(2,1)} async-done(((bf16[1,256,512]{2,1,0:T(8,128)(2,1)}), bf16[4,256,512]{2,1,0:T(8,128)(2,1)}) %all-gather.2.cloned.1.call-update) | async-done | bytes 1048592 | tf_op jit(solution)/shard_map/all_gather | solution.py:33
  51.0 1.5 %copy.12 = bf16[4,256,512]{1,2,0:T(8,128)(2,1)S(1)} copy(bf16[4,256,512]{2,1,0:T(8,128)(2,1)} %all-gather.2.cloned.1.call-done) | data formatting | bytes 2097152 | tf_op jit(solution)/shard_map/all_gather | solution.py:33
  52.5 3.5 %fusion.4 = f32[256,1024]{1,0:T(8,128)S(1)} fusion(bf16[256,2048]{0,1:T(8,128)(2,1)S(1)} %bitcast.43, bf16[1,2048,1024]{2,1,0:T(8,128)(2,1)} %param.10), kind=kOutput, calls=%fused_computation.5 | convolution fusion | flops 1073741824 | bytes 6291456 | tf_op jit(solution)/shard_map/dot_general | solution.py:34
  56.0 6.9 %fusion.9 = bf16[2048,256]{0,1:T(8,128)(2,1)} fusion(bf16[1,1024,2048]{2,1,0:T(8,128)(2,1)} %param.12, bf16[256,2048]{0,1:T(8,128)(2,1)S(1)} %bitcast.44, bf16[1,2048,1024]{2,1,0:T(8,128)(2,1)} %param.11, f32[256,1024]{1,0:T(8,128)S(1)} %fusion.4), kind=kOutput, calls=%fused_computation.8 | convolution fusion | flops 2149580800 | bytes 11534336 | tf_op jit(solution)/shard_map/dot_general | solution.py:38
  62.9 0.0 reduce-scatter.2.cloned.1.call-update
  62.9 0.1 eq.15
  63.0 0.1 mul.35
  63.1 1.8 %multiply_convert_fusion = bf16[256,256]{1,0:T(8,128)(2,1)S(1)} fusion(bf16[256,2048]{1,0:T(8,128)(2,1)S(1)} %copy-done, bf16[2048,256]{1,0:T(8,128)(2,1)} %param.13), kind=kOutput, calls=%fused_computation.20 | convolution fusion | flops 268763136 | bytes 2228224 | tf_op jit(solution)/shard_map/dot_general | solution.py:57
  64.9 17.9 %all_gather.7 = bf16[256,1024]{1,0:T(8,128)(2,1)S(1)} all-gather(bf16[256,256]{1,0:T(8,128)(2,1)S(1)} %multiply_convert_fusion), channel_id=1, replica_groups=mesh['ep'=8,'tp'=4] {'tp'}, dimensions={1}, use_global_device_ids=true | all-gather | bytes 655360 | tf_op jit(solution)/shard_map/all_gather | solution.py:60
  82.8 11.8 %reduce-scatter.2.cloned.1.call-done = bf16[512,256]{0,1:T(8,128)(2,1)} async-done(((bf16[2048,256]{0,1:T(8,128)(2,1)}), bf16[512,256]{0,1:T(8,128)(2,1)}) %reduce-scatter.2.cloned.1.call-update) | async-done | bytes 262160 | tf_op jit(solution)/shard_map/reduce_scatter | solution.py:37
  94.6 4.6 %all-to-all-start.1 = ((bf16[512,8,32]{0,2,1:T(8,128)(2,1)}), bf16[512,8,32]{0,2,1:T(8,128)(2,1)S(1)}, u32[]{:S(2)}, u32[]{:S(2)}) async-start(bf16[512,8,32]{0,2,1:T(8,128)(2,1)} %bitcast.46), calls=%async_computation.2 | async-start | bytes 524288 | tf_op jit(solution)/shard_map/all_to_all | solution.py:45
  99.2 0.4 fusion.32
  99.6 9.3 %all-to-all-done.1 = bf16[512,8,32]{0,2,1:T(8,128)(2,1)S(1)} async-done(((bf16[512,8,32]{0,2,1:T(8,128)(2,1)}), bf16[512,8,32]{0,2,1:T(8,128)(2,1)S(1)}, u32[]{:S(2)}, u32[]{:S(2)}) %all-to-all-start.1) | async-done | bytes 262176 | tf_op jit(solution)/shard_map/all_to_all | solution.py:45
  108.9 0.1 fusion.23
  109.0 0.3 fusion.28
  109.4 0.4 convolution_add_fusion
  109.8 1.1 fusion.19
  (16 shorter events, 0.1 us)
Async XLA Ops:
  6.5 1.6 %copy-start = (bf16[256,2048]{1,0:T(8,128)(2,1)S(1)}, bf16[256,2048]{1,0:T(8,128)(2,1)}, u32[]{:S(2)}) copy-start(bf16[256,2048]{1,0:T(8,128)(2,1)} %param.9) | copy-start | bytes 3145732
  6.5 44.5 %all-gather.2.cloned.1.call-start = ((), (), s32[]{:S(2)}) async-start(), calls=%async_computation.3 | async-start | bytes 1310720 | tf_op jit(solution)/shard_map/all_gather | solution.py:33
  25.4 69.2 %reduce-scatter.2.cloned.1.call-start = ((), (), s32[]{:S(2)}) async-start(), calls=%async_computation.4 | async-start | bytes 1310720 | tf_op jit(solution)/shard_map/reduce_scatter | solution.py:37
  55.9 7.0 %copy-start.2 = (s32[8,32]{1,0:T(8,128)S(1)}, s32[8,32]{1,0:T(8,128)}, u32[]{:S(2)}) copy-start(s32[8,32]{1,0:T(8,128)} %param.16) | copy-start | bytes 3076
  55.9 7.1 %copy-start.4 = (f32[8,32]{1,0:T(8,128)S(1)}, f32[8,32]{1,0:T(8,128)}, u32[]{:S(2)}) copy-start(f32[8,32]{1,0:T(8,128)} %param.17) | copy-start | bytes 3076
  56.0 7.1 %copy-start.3 = (bf16[2048]{0:T(1024)(128)(2,1)S(1)}, bf16[2048]{0:T(1024)(128)(2,1)}, u32[]{:S(2)}) copy-start(bf16[2048]{0:T(1024)(128)(2,1)} %param.15) | copy-start | bytes 12292
  63.1 46.7 %copy-start.1 = (bf16[1024,512]{1,0:T(8,128)(2,1)S(1)}, bf16[1024,512]{1,0:T(8,128)(2,1)}, u32[]{:S(2)}) copy-start(bf16[1024,512]{1,0:T(8,128)(2,1)} %param.14) | copy-start | bytes 3145732
  94.6 14.3 %all-to-all-start.1 = ((bf16[512,8,32]{0,2,1:T(8,128)(2,1)}), bf16[512,8,32]{0,2,1:T(8,128)(2,1)S(1)}, u32[]{:S(2)}, u32[]{:S(2)}) async-start(bf16[512,8,32]{0,2,1:T(8,128)(2,1)} %bitcast.46), calls=%async_computation.2 | async-start | bytes 524288 | tf_op jit(solution)/shard_map/all_to_all | solution.py:45
Sparse Core Ops, SparseCore 0:
  25.5 25.4 all-gather.1
  63.0 31.4 reduce-scatter.1
